TPU v7x, 32 devices: a whole 2x2x4 slice. The times are simulated.
32 devices in a mesh: sp: 8 (over z, x), dp: 4 (over y, core).
Axes of the slice: x: 2, y: 2, z: 4, core: 2. Of those that a mesh axis runs over, the one named last changes fastest.
Arguments:
- queries: bfloat16 [16, 8, 512, 256], P('dp', None, 'sp'), may hold values from -6 to 6
- keys: bfloat16 [16, 8, 512, 256], P('dp', None, 'sp'), may hold values from -6 to 6
- values: bfloat16 [16, 8, 512, 256], P('dp', None, 'sp'), may hold values from -6 to 6
- log_decay: float32 [128, 512], P(('dp', 'sp')), may hold values from -2 to 0, as said below
- w_out: bfloat16 [8, 256, 2048], P(None, None, 'dp'), may hold values from -0.125 to 0.125
Outputs:
- mixed_out: bfloat16 [16, 512, 2048], P('dp', 'sp')
Inputs may be any that keep to these rules, and one draw needn't show every extreme that they name: Every entry of log_decay is below zero.
All inputs are finite; a program needn't handle non-finite values.
Results may differ from a plain program's by a relative error of at most 0.008.
Values may be sent and summed in bfloat16 or wider, within the bound.
A program may use at most 128 MiB of HBM per device.

v0:
```python
import jax
import jax.numpy as jnp
from jax import lax
from jax.sharding import PartitionSpec as P

BLOCK = 64


def rotate(field_in, cosine, sine_tab):
    half_dim = field_in.shape[1] // 2
    widened = field_in.astype(jnp.float32)
    first_half = widened[:, :half_dim]
    second_half = widened[:, half_dim:]
    turned = jnp.concatenate(
        [
            first_half * cosine - second_half * sine_tab,
            second_half * cosine + first_half * sine_tab,
        ],
        axis=1,
    )
    return turned.astype(jnp.bfloat16)


def retain(query_rows, key_rows, value_rows, decay_row, cosine, sine_tab):
    length, head_width = query_rows.shape
    blocks = length // BLOCK
    rot_query = rotate(query_rows, cosine, sine_tab).reshape(blocks, BLOCK, head_width)
    rot_key = rotate(key_rows, cosine, sine_tab).reshape(blocks, BLOCK, head_width)
    value_blocks = value_rows.reshape(blocks, BLOCK, head_width)
    within = jnp.cumsum(decay_row.reshape(blocks, BLOCK), axis=1)
    ending = within[:, -1:]
    causal = jnp.tril(jnp.ones((BLOCK, BLOCK), dtype=bool))[None]
    spread = within[:, :, None] - within[:, None, :]
    decay_mask = jnp.where(causal, jnp.exp(jnp.where(causal, spread, 0.0)), 0.0)
    scores = jnp.einsum("bnd,bmd->bnm", rot_query, rot_key, preferred_element_type=jnp.float32)
    weights = (scores * decay_mask).astype(jnp.bfloat16)
    scaled_keys = (rot_key * jnp.exp(ending - within)[:, :, None]).astype(jnp.bfloat16)
    updates = jnp.einsum(
        "bmd,bme->bde", scaled_keys, value_blocks, preferred_element_type=jnp.float32
    )

    def advance(state_now, inputs):
        factor, update = inputs
        return (factor * state_now + update, state_now.astype(jnp.bfloat16))

    start_state = jnp.zeros((head_width, head_width), jnp.float32)
    _, before = lax.scan(advance, start_state, (jnp.exp(ending[:, 0]), updates))
    local_part = jnp.einsum(
        "bnm,bme->bne", weights, value_blocks, preferred_element_type=jnp.float32
    )
    carried = jnp.einsum("bnd,bde->bne", rot_query, before, preferred_element_type=jnp.float32)
    combined = local_part + jnp.exp(within)[:, :, None] * carried
    return combined.reshape(length, head_width).astype(jnp.bfloat16)


def on_device(queries, keys, values, log_decay, w_out):
    groups, head_count, seg_len, head_width = queries.shape
    item_count = groups * head_count
    flat_q = queries.reshape(item_count, seg_len, head_width)
    flat_k = keys.reshape(item_count, seg_len, head_width)
    flat_v = values.reshape(item_count, seg_len, head_width)
    head_k, head_v = (
        lax.all_to_all(flat_k, "sp", split_axis=0, concat_axis=1, tiled=True),
        lax.all_to_all(flat_v, "sp", split_axis=0, concat_axis=1, tiled=True),
    )
    head_q = lax.all_to_all(flat_q, "sp", split_axis=0, concat_axis=1, tiled=True)
    length = head_q.shape[1]
    half_dim = head_width // 2
    frequency = 10000.0 ** (-jnp.arange(half_dim, dtype=jnp.float32) / half_dim)
    angles = jnp.arange(length, dtype=jnp.float32)[:, None] * frequency[None, :]
    cosine = jnp.cos(angles)
    sine_tab = jnp.sin(angles)

    def one_item(inputs):
        return retain(inputs[0], inputs[1], inputs[2], inputs[3], cosine, sine_tab)

    retained = lax.map(one_item, (head_q, head_k, head_v, log_decay))
    by_token = lax.all_to_all(retained, "sp", split_axis=1, concat_axis=0, tiled=True)
    by_token = by_token.reshape(groups, head_count, seg_len, head_width)
    widened = by_token.astype(jnp.float32)
    normed = (
        widened * lax.rsqrt(jnp.mean(widened * widened, axis=-1, keepdims=True) + 1e-06)
    ).astype(jnp.bfloat16)
    mixed_out = jnp.einsum(
        "shtd,hde->ste",
        normed,
        lax.all_gather(w_out, "dp", axis=2, tiled=True),
        preferred_element_type=jnp.float32,
    )
    return mixed_out.astype(jnp.bfloat16)


def solution(mesh):
    placed = (
        P("dp", None, "sp", None),
        P("dp", None, "sp", None),
        P("dp", None, "sp", None),
        P(("dp", "sp"), None),
        P(None, None, "dp"),
    )
    return jax.shard_map(
        on_device, mesh=mesh, in_specs=placed, out_specs=P("dp", "sp", None), check_vma=False
    )
```

profile of v0, /device:TPU:0, one launch (start us, length us, event | category | flops | bytes accessed | tf_op | source)
XLA Modules:
  0.0 242.2 jit_solution(14307589264207442078)
XLA Ops:
  6.5 33.2 %all_to_all.63 = bf16[32,64,256]{2,1,0:T(8,128)(2,1)S(1)} all-to-all(bf16[32,64,256]{2,1,0:T(8,128)(2,1)} %bitcast.108), channel_id=1, replica_groups=mesh['sp'=8,'dp'=4] {'sp'}, dimensions={0} | all-to-all | bytes 2097152 | tf_op jit(solution)/shard_map/all_to_all | solution.py:64
  39.7 28.8 %all_to_all.64 = bf16[32,64,256]{2,1,0:T(8,128)(2,1)S(1)} all-to-all(bf16[32,64,256]{2,1,0:T(8,128)(2,1)S(1)} %bitcast.109), channel_id=1, replica_groups=mesh['sp'=8,'dp'=4] {'sp'}, dimensions={0} | all-to-all | bytes 2097152 | tf_op jit(solution)/shard_map/all_to_all | solution.py:66
  68.6 3.6 %all-to-all-start.1 = ((bf16[32,64,256]{2,1,0:T(8,128)(2,1)}), bf16[32,64,256]{2,1,0:T(8,128)(2,1)S(1)}, u32[]{:S(2)}, u32[]{:S(2)}) async-start(bf16[32,64,256]{2,1,0:T(8,128)(2,1)} %bitcast.110), calls=%async_computation.1 | async-start | bytes 2097152 | tf_op jit(solution)/shard_map/all_to_all | solution.py:63
  72.9 1.0 copy.28
  73.9 1.1 copy.26
  75.1 22.6 %all-to-all-done.1 = bf16[32,64,256]{2,1,0:T(8,128)(2,1)S(1)} async-done(((bf16[32,64,256]{2,1,0:T(8,128)(2,1)}), bf16[32,64,256]{2,1,0:T(8,128)(2,1)S(1)}, u32[]{:S(2)}, u32[]{:S(2)}) %all-to-all-start.1) | async-done | bytes 1048608 | tf_op jit(solution)/shard_map/all_to_all | solution.py:63
  97.6 1.0 copy.27
  98.7 97.2 %while.30 = (s32[]{:T(128)}, bf16[4,512,256]{2,1,0:T(8,128)(2,1)}, bf16[4,512,256]{2,1,0:T(8,128)(2,1)}, bf16[4,512,256]{2,1,0:T(8,128)(2,1)}, f32[4,512]{1,0:T(...) while((s32[]{:T(128)}, bf16[4,512,256]{2,1,0:T(8,128)(2,1)}, ...), condition=%wide.region_4.5_spmd.clone.clone.clone, body=%wide.region_0.4_spmd.clone.clone.clone.sunk | while | flops 172363776 | bytes 15632365 | solution.py:77
  98.7 1.1 bitcast_convert_fusion.3
  99.8 1.2 fusion.70
  104.0 16.7 %while.31 = (s32[]{:T(128)}, f32[256,256]{1,0:T(8,128)S(1)}, bf16[8,256,256]{2,1,0:T(8,128)(2,1)}, f32[8]{0:T(128)S(1)}, f32[8,256,256]{2,1,0:T(8,128)S(1)}, /*index=5*/s32[]{:T(128)}, s32[]{:T(128)}) while((s32[]{:T(128)}, f32[256,256]{1,0:T(8,128)S(1)}, bf16[8,256,256]{2,1,0:T(8,128)(2,1)}, f32[8]{0:T(128)S(1)}, ...), condition=%wide.region_3.3_spmd.clone, body=%wide.region_2.2_spmd.clone.sunk | while | flops 262147 | bytes 1180268 | solution.py:47
  123.0 1.1 bitcast_convert_fusion.3
  124.1 1.2 fusion.70
  126.6 1.0 constant_dynamic-slice_fusion.2
  128.3 16.7 %while.31 = (s32[]{:T(128)}, f32[256,256]{1,0:T(8,128)S(1)}, bf16[8,256,256]{2,1,0:T(8,128)(2,1)}, f32[8]{0:T(128)S(1)}, f32[8,256,256]{2,1,0:T(8,128)S(1)}, /*index=5*/s32[]{:T(128)}, s32[]{:T(128)}) while((s32[]{:T(128)}, f32[256,256]{1,0:T(8,128)S(1)}, bf16[8,256,256]{2,1,0:T(8,128)(2,1)}, f32[8]{0:T(128)S(1)}, ...), condition=%wide.region_3.3_spmd.clone, body=%wide.region_2.2_spmd.clone.sunk | while | flops 262147 | bytes 1180268 | solution.py:47
  147.3 1.1 bitcast_convert_fusion.3
  148.4 1.2 fusion.70
  152.6 16.7 %while.31 = (s32[]{:T(128)}, f32[256,256]{1,0:T(8,128)S(1)}, bf16[8,256,256]{2,1,0:T(8,128)(2,1)}, f32[8]{0:T(128)S(1)}, f32[8,256,256]{2,1,0:T(8,128)S(1)}, /*index=5*/s32[]{:T(128)}, s32[]{:T(128)}) while((s32[]{:T(128)}, f32[256,256]{1,0:T(8,128)S(1)}, bf16[8,256,256]{2,1,0:T(8,128)(2,1)}, f32[8]{0:T(128)S(1)}, ...), condition=%wide.region_3.3_spmd.clone, body=%wide.region_2.2_spmd.clone.sunk | while | flops 262147 | bytes 1180268 | solution.py:47
  171.6 1.1 bitcast_convert_fusion.3
  172.7 1.2 fusion.70
  176.9 16.7 %while.31 = (s32[]{:T(128)}, f32[256,256]{1,0:T(8,128)S(1)}, bf16[8,256,256]{2,1,0:T(8,128)(2,1)}, f32[8]{0:T(128)S(1)}, f32[8,256,256]{2,1,0:T(8,128)S(1)}, /*index=5*/s32[]{:T(128)}, s32[]{:T(128)}) while((s32[]{:T(128)}, f32[256,256]{1,0:T(8,128)S(1)}, bf16[8,256,256]{2,1,0:T(8,128)(2,1)}, f32[8]{0:T(128)S(1)}, ...), condition=%wide.region_3.3_spmd.clone, body=%wide.region_2.2_spmd.clone.sunk | while | flops 262147 | bytes 1180268 | solution.py:47
  195.9 2.0 copy.29
  198.0 29.1 %all_to_all.65 = bf16[4,512,256]{2,0,1:T(4,128)(2,1)S(1)} all-to-all(bf16[4,512,256]{2,0,1:T(4,128)(2,1)S(1)} %copy.29), channel_id=1, replica_groups=mesh['sp'=8,'dp'=4] {'sp'}, dimensions={1} | all-to-all | bytes 2097152 | tf_op jit(solution)/shard_map/all_to_all | solution.py:78
  228.5 6.8 %fusion.48 = bf16[4,64,2048]{2,1,0:T(8,128)(2,1)} fusion(bf16[8,256,2048]{2,1,0:T(8,128)(2,1)} %all-gather.2.cloned.1.call-done, f32[4,8,64]{2,1,0:T(8,128)S(1)} %bitcast.112, f32[4,8,64,256]{3,2,1,0:T(8,128)S(1)} %bitcast.107), kind=kOutput, calls=%fused_computation.59 | convolution fusion | flops 2149056512 | bytes 11542528 | tf_op jit(solution)/shard_map/shtd,hde->ste/dot_general | solution.py:84
  (171 shorter events, 88.4 us)
Async XLA Ops:
  6.5 33.2 %copy-start.1 = (bf16[4,8,64,256]{3,2,1,0:T(8,128)(2,1)S(1)}, bf16[4,8,64,256]{3,2,1,0:T(8,128)(2,1)}, u32[]{:S(2)}) copy-start(bf16[4,8,64,256]{3,2,1,0:T(8,128)(2,1)} %param.9) | copy-start | bytes 3145732
  68.6 29.1 %all-to-all-start.1 = ((bf16[32,64,256]{2,1,0:T(8,128)(2,1)}), bf16[32,64,256]{2,1,0:T(8,128)(2,1)S(1)}, u32[]{:S(2)}, u32[]{:S(2)}) async-start(bf16[32,64,256]{2,1,0:T(8,128)(2,1)} %bitcast.110), calls=%async_computation.1 | async-start | bytes 2097152 | tf_op jit(solution)/shard_map/all_to_all | solution.py:63
  72.1 156.4 %all-gather.2.cloned.1.call-start = ((), (), s32[]{:S(2)}) async-start(), calls=%async_computation.4 | async-start | bytes 10485760 | tf_op jit(solution)/shard_map/all_gather | solution.py:87
  120.7 1.2 copy-start
  145.0 1.2 copy-start
  169.3 1.2 copy-start
  193.7 1.2 copy-start
Sparse Core Ops, SparseCore 0:
  74.5 59.6 all-gather.1
where the time goes:
time: 243 us; the launch traced here: 242 us
  blocking collectives  91.1 us (37%)
  other arithmetic  56.7 us (23%)
  local copies, waits for them, and re-layouts  40.7 us (17%)
  waiting for transfers between devices  23.3 us (10%)
  between operations  13.5 us (6%)
  matrix products  12.3 us (5%)
  starting transfers between devices  3.6 us (1%)
    all_to_all x1, blocking collectives, on_device(): lax.all_to_all(flat_v, 'sp', split_axis=0, concat_axis=1, tiled=True)  33.2 us
    all_to_all x1, blocking collectives, on_device(): lax.all_to_all(retained, 'sp', split_axis=1, concat_axis=0, tiled=True)  29.1 us
    all_to_all x1, blocking collectives, on_device(): lax.all_to_all(flat_q, 'sp', split_axis=0, concat_axis=1, tiled=True)  28.8 us
    add x32, other arithmetic, advance(): return (factor * state_now + update, state_now.astype(jnp.bfloat16))  24 us
    all_to_all x1, waiting for transfers between devices, on_device(): lax.all_to_all(flat_k, 'sp', split_axis=0, concat_axis=1, tiled=True)  22.6 us
    dynamic_update_slice x32, other arithmetic, retain(): _, before = lax.scan(advance, start_state, (jnp.exp(ending[:, 0]), updates))  21.5 us
    dynamic_slice x32, local copies, waits for them, and re-layouts, retain(): _, before = lax.scan(advance, start_state, (jnp.exp(ending[:, 0]), updates))  20.7 us
    dynamic_slice x8, local copies, waits for them, and re-layouts, on_device(): retained = lax.map(one_item, (head_q, head_k, head_v, log_decay))  6.8 us
  transfers between devices with their start and end apart: 2, of which 1 were waited for; matrix products, arithmetic and copies ran while one was open for 41% of the time, Pallas kernels for 0%

commit v1 on v0

--- a/solution.py
+++ b/solution.py
@@ -4,6 +4,29 @@
 from jax.sharding import PartitionSpec as P
 
 BLOCK = 64
+
+
+def in_blocks(x, dim, peers):
+    shape = x.shape
+    blocks = x.reshape(*shape[:dim], peers, shape[dim] // peers, *shape[dim + 1 :])
+    return jnp.moveaxis(blocks, dim, 0)
+
+
+def in_order(blocks, dim):
+    shape = list(blocks.shape[1:])
+    shape[dim] *= blocks.shape[0]
+    return jnp.moveaxis(blocks, 0, dim).reshape(shape)
+
+
+def pairwise_exchange(x, axis, split_dim, concat_dim):
+    count, here = (lax.axis_size(axis), lax.axis_index(axis))
+    blocks = in_blocks(x, split_dim, count)
+    outs = [blocks[here]]
+    for hop in range(1, count):
+        sent = blocks[here ^ hop]
+        outs.append(lax.ppermute(sent, axis, [(i, i ^ hop) for i in range(count)]))
+    blocks = jnp.stack(outs)[here ^ jnp.arange(count)]
+    return in_order(blocks, concat_dim)
 
 
 def rotate(field_in, cosine, sine_tab):
@@ -61,7 +84,7 @@
     flat_v = values.reshape(item_count, seg_len, head_width)
     head_k, head_v = (
         lax.all_to_all(flat_k, "sp", split_axis=0, concat_axis=1, tiled=True),
-        lax.all_to_all(flat_v, "sp", split_axis=0, concat_axis=1, tiled=True),
+        pairwise_exchange(flat_v, "sp", 0, 1),
     )
     head_q = lax.all_to_all(flat_q, "sp", split_axis=0, concat_axis=1, tiled=True)
     length = head_q.shape[1]

time: 243 us -> 231 us (0.951)
  blocking collectives: 91.1 us -> 37.4 us
  starting transfers between devices: 3.6 us -> 24 us
  waiting for transfers between devices: 23.3 us -> 39.4 us
  local copies, waits for them, and re-layouts: 40.7 us -> 46.9 us
    all_to_all x2 -> x0, blocking collectives: 62 us -> none  [the longest x1 33.2 us: on_device(): lax.all_to_all(flat_v, 'sp', split_axis=0, concat_axis=1, tiled=True)]
    all_to_all x0 -> x1, waiting for transfers between devices: none -> 24 us  [on_device(): lax.all_to_all(flat_q, 'sp', split_axis=0, concat_axis=1, tiled=True)]
    all_to_all x1, waiting for transfers between devices: 22.6 us -> 3.22 us  [on_device(): lax.all_to_all(flat_k, 'sp', split_axis=0, concat_axis=1, tiled=True)]
    ppermute x0 -> x7, starting transfers between devices: none -> 13 us  [pairwise_exchange(): outs.append(lax.ppermute(sent, axis, [(i, i ^ hop) for i in range(count)]))]
    ppermute x0 -> x7, waiting for transfers between devices: none -> 12.1 us  [pairwise_exchange(): outs.append(lax.ppermute(sent, axis, [(i, i ^ hop) for i in range(count)]))]
    all_to_all x1, blocking collectives: 29.1 us -> 37.4 us  [on_device(): lax.all_to_all(retained, 'sp', split_axis=1, concat_axis=0, tiled=True)]
    all_to_all x0 -> x1, starting transfers between devices: none -> 7.41 us  [on_device(): lax.all_to_all(flat_q, 'sp', split_axis=0, concat_axis=1, tiled=True)]
    unnamed x2 -> x8, local copies, waits for them, and re-layouts: 0.01 us -> 4.88 us
  transfers between devices with their start and end apart: 2 -> 10, of which waited for: 1 -> 5; matrix products, arithmetic and copies ran while one was open for 41% -> 45% of each run, Pallas kernels for 0% -> 0%
where the time goes in v1:
time: 231 us; the launch traced here: 229 us
  other arithmetic  54.9 us (24%)
  local copies, waits for them, and re-layouts  46.9 us (20%)
  waiting for transfers between devices  39.4 us (17%)
  blocking collectives  37.4 us (16%)
  starting transfers between devices  24 us (10%)
  between operations  13.5 us (6%)
  matrix products  12.2 us (5%)
    all_to_all x1, blocking collectives, on_device(): lax.all_to_all(retained, 'sp', split_axis=1, concat_axis=0, tiled=True)  37.4 us
    all_to_all x1, waiting for transfers between devices, on_device(): lax.all_to_all(flat_q, 'sp', split_axis=0, concat_axis=1, tiled=True)  24 us
    add x32, other arithmetic, advance(): return (factor * state_now + update, state_now.astype(jnp.bfloat16))  22.1 us
    dynamic_update_slice x32, other arithmetic, retain(): _, before = lax.scan(advance, start_state, (jnp.exp(ending[:, 0]), updates))  21.5 us
    dynamic_slice x32, local copies, waits for them, and re-layouts, retain(): _, before = lax.scan(advance, start_state, (jnp.exp(ending[:, 0]), updates))  18.8 us
    ppermute x7, starting transfers between devices, pairwise_exchange(): outs.append(lax.ppermute(sent, axis, [(i, i ^ hop) for i in range(count)]))  13 us
    ppermute x7, waiting for transfers between devices, pairwise_exchange(): outs.append(lax.ppermute(sent, axis, [(i, i ^ hop) for i in range(count)]))  12.1 us
    all_to_all x1, starting transfers between devices, on_device(): lax.all_to_all(flat_q, 'sp', split_axis=0, concat_axis=1, tiled=True)  7.41 us
  transfers between devices with their start and end apart: 10, of which 5 were waited for; matrix products, arithmetic and copies ran while one was open for 45% of the time, Pallas kernels for 0%

profile of v1, /device:TPU:0, one launch (start us, length us, event | category | flops | bytes accessed | tf_op | source)
XLA Modules:
  0.0 229.4 jit_solution(11022641974284253689)
XLA Ops:
  6.5 7.4 %all-to-all-start = ((bf16[32,64,256]{2,1,0:T(8,128)(2,1)}), bf16[32,64,256]{2,1,0:T(8,128)(2,1)S(1)}, u32[]{:S(2)}, u32[]{:S(2)}) async-start(bf16[32,64,256]{2,1,0:T(8,128)(2,1)} %bitcast.137), calls=%async_computation | async-start | bytes 2097152 | tf_op jit(solution)/shard_map/all_to_all | solution.py:89
  14.8 1.9 collective-permute-start
  16.8 1.5 collective-permute-start.1
  18.3 2.8 %collective-permute-start.3 = (bf16[4,64,256]{2,1,0:T(8,128)(2,1)S(1)}, bf16[4,64,256]{2,1,0:T(8,128)(2,1)S(1)}, u32[]{:S(2)}, u32[]{:S(2)}) collective-permute-start(bf16[4,64,256]{2,1,0:T(8,128)(2,1)S(1)} %get-tuple-element.223), channel_id=1, source_target_pairs={{0,16},{4,20},{8,24},{12,28},{16,0},{20,4},{24,8},{28,12},{1,17},{... | collective-permute-start | bytes 393224 | tf_op jit(solution)/shard_map/ppermute | solution.py:27
  21.2 1.5 collective-permute-start.4
  22.7 24.0 %all-to-all-done = bf16[32,64,256]{2,1,0:T(8,128)(2,1)S(1)} async-done(((bf16[32,64,256]{2,1,0:T(8,128)(2,1)}), bf16[32,64,256]{2,1,0:T(8,128)(2,1)S(1)}, u32[]{:S(2)}, u32[]{:S(2)}) %all-to-all-start) | async-done | bytes 1048608 | tf_op jit(solution)/shard_map/all_to_all | solution.py:89
  46.7 3.6 %all-to-all-start.1 = ((bf16[32,64,256]{2,1,0:T(8,128)(2,1)}), bf16[32,64,256]{2,1,0:T(8,128)(2,1)S(1)}, u32[]{:S(2)}, u32[]{:S(2)}) async-start(bf16[32,64,256]{2,1,0:T(8,128)(2,1)} %bitcast.4), calls=%async_computation.1 | async-start | bytes 2097152 | tf_op jit(solution)/shard_map/all_to_all | solution.py:86
  50.3 3.8 %collective-permute-start.5 = (bf16[4,64,256]{2,1,0:T(8,128)(2,1)S(1)}, bf16[4,64,256]{2,1,0:T(8,128)(2,1)S(1)}, u32[]{:S(2)}, u32[]{:S(2)}) collective-permute-start(bf16[4,64,256]{2,1,0:T(8,128)(2,1)S(1)} %get-tuple-element.221), channel_id=1, source_target_pairs={{0,24},{4,28},{8,16},{12,20},{16,8},{20,12},{24,0},{28,4},{1,25},{... | collective-permute-start | bytes 393224 | tf_op jit(solution)/shard_map/ppermute | solution.py:27
  54.1 1.6 bitcast_dynamic-update-slice_fusion.7
  55.7 1.4 collective-permute-start.6
  60.5 9.7 %collective-permute-done.5 = bf16[4,64,256]{2,1,0:T(8,128)(2,1)S(1)} collective-permute-done((bf16[4,64,256]{2,1,0:T(8,128)(2,1)S(1)}, bf16[4,64,256]{2,1,0:T(8,128)(2,1)S(1)}, u32[]{:S(2)}, u32[]{:S(2)}) %collective-permute-start.5) | collective-permute-done | bytes 131104 | tf_op jit(solution)/shard_map/ppermute | solution.py:27
  70.8 1.8 collective-permute-done.6
  73.2 1.8 gather_fusion
  77.3 3.2 %all-to-all-done.1 = bf16[32,64,256]{2,1,0:T(8,128)(2,1)S(1)} async-done(((bf16[32,64,256]{2,1,0:T(8,128)(2,1)}), bf16[32,64,256]{2,1,0:T(8,128)(2,1)S(1)}, u32[]{:S(2)}, u32[]{:S(2)}) %all-to-all-start.1) | async-done | bytes 1048608 | tf_op jit(solution)/shard_map/all_to_all | solution.py:86
  81.5 93.5 %while.30 = (s32[]{:T(128)}, bf16[4,512,256]{2,1,0:T(8,128)(2,1)}, bf16[4,512,256]{2,1,0:T(8,128)(2,1)}, bf16[4,512,256]{2,1,0:T(8,128)(2,1)}, f32[4,512]{1,0:T(...) while((s32[]{:T(128)}, bf16[4,512,256]{2,1,0:T(8,128)(2,1)}, ...), condition=%wide.region_4.5_spmd.clone.clone.clone, body=%wide.region_0.4_spmd.clone.clone.clone.sunk | while | flops 172363776 | bytes 15632365 | solution.py:100
  86.8 15.8 %while.31 = (s32[]{:T(128)}, f32[256,256]{1,0:T(8,128)S(1)}, bf16[8,256,256]{2,1,0:T(8,128)(2,1)}, f32[8]{0:T(128)S(1)}, f32[8,256,256]{2,1,0:T(8,128)S(1)}, /*index=5*/s32[]{:T(128)}, s32[]{:T(128)}) while((s32[]{:T(128)}, f32[256,256]{1,0:T(8,128)S(1)}, bf16[8,256,256]{2,1,0:T(8,128)(2,1)}, f32[8]{0:T(128)S(1)}, ...), condition=%wide.region_3.3_spmd.clone, body=%wide.region_2.2_spmd.clone.sunk | while | flops 262147 | bytes 1180268 | solution.py:70
  106.0 1.2 fusion.71
  110.2 15.8 %while.31 = (s32[]{:T(128)}, f32[256,256]{1,0:T(8,128)S(1)}, bf16[8,256,256]{2,1,0:T(8,128)(2,1)}, f32[8]{0:T(128)S(1)}, f32[8,256,256]{2,1,0:T(8,128)S(1)}, /*index=5*/s32[]{:T(128)}, s32[]{:T(128)}) while((s32[]{:T(128)}, f32[256,256]{1,0:T(8,128)S(1)}, bf16[8,256,256]{2,1,0:T(8,128)(2,1)}, f32[8]{0:T(128)S(1)}, ...), condition=%wide.region_3.3_spmd.clone, body=%wide.region_2.2_spmd.clone.sunk | while | flops 262147 | bytes 1180268 | solution.py:70
  129.4 1.2 fusion.71
  133.6 15.8 %while.31 = (s32[]{:T(128)}, f32[256,256]{1,0:T(8,128)S(1)}, bf16[8,256,256]{2,1,0:T(8,128)(2,1)}, f32[8]{0:T(128)S(1)}, f32[8,256,256]{2,1,0:T(8,128)S(1)}, /*index=5*/s32[]{:T(128)}, s32[]{:T(128)}) while((s32[]{:T(128)}, f32[256,256]{1,0:T(8,128)S(1)}, bf16[8,256,256]{2,1,0:T(8,128)(2,1)}, f32[8]{0:T(128)S(1)}, ...), condition=%wide.region_3.3_spmd.clone, body=%wide.region_2.2_spmd.clone.sunk | while | flops 262147 | bytes 1180268 | solution.py:70
  156.9 15.8 %while.31 = (s32[]{:T(128)}, f32[256,256]{1,0:T(8,128)S(1)}, bf16[8,256,256]{2,1,0:T(8,128)(2,1)}, f32[8]{0:T(128)S(1)}, f32[8,256,256]{2,1,0:T(8,128)S(1)}, /*index=5*/s32[]{:T(128)}, s32[]{:T(128)}) while((s32[]{:T(128)}, f32[256,256]{1,0:T(8,128)S(1)}, bf16[8,256,256]{2,1,0:T(8,128)(2,1)}, f32[8]{0:T(128)S(1)}, ...), condition=%wide.region_3.3_spmd.clone, body=%wide.region_2.2_spmd.clone.sunk | while | flops 262147 | bytes 1180268 | solution.py:70
  175.0 2.0 copy.29
  177.0 37.4 %all_to_all.45 = bf16[4,512,256]{2,0,1:T(4,128)(2,1)S(1)} all-to-all(bf16[4,512,256]{2,0,1:T(4,128)(2,1)S(1)} %copy.29), channel_id=1, replica_groups=mesh['sp'=8,'dp'=4] {'sp'}, dimensions={1} | all-to-all | bytes 2097152 | tf_op jit(solution)/shard_map/all_to_all | solution.py:101
  215.9 6.7 %fusion.48 = bf16[4,64,2048]{2,1,0:T(8,128)(2,1)} fusion(bf16[8,256,2048]{2,1,0:T(8,128)(2,1)} %all-gather.2.cloned.1.call-done, f32[4,8,64]{2,1,0:T(8,128)S(1)} %bitcast.139, f32[4,8,64,256]{3,2,1,0:T(8,128)S(1)} %bitcast.135), kind=kOutput, calls=%fused_computation.60 | convolution fusion | flops 2149056512 | bytes 11542528 | tf_op jit(solution)/shard_map/shtd,hde->ste/dot_general | solution.py:107
  (196 shorter events, 100.4 us)
Async XLA Ops:
  6.5 7.5 %copy-start.1 = (bf16[4,8,64,256]{3,2,1,0:T(8,128)(2,1)S(1)}, bf16[4,8,64,256]{3,2,1,0:T(8,128)(2,1)}, u32[]{:S(2)}) copy-start(bf16[4,8,64,256]{3,2,1,0:T(8,128)(2,1)} %param.11) | copy-start | bytes 3145732
  6.5 40.2 %all-to-all-start = ((bf16[32,64,256]{2,1,0:T(8,128)(2,1)}), bf16[32,64,256]{2,1,0:T(8,128)(2,1)S(1)}, u32[]{:S(2)}, u32[]{:S(2)}) async-start(bf16[32,64,256]{2,1,0:T(8,128)(2,1)} %bitcast.137), calls=%async_computation | async-start | bytes 2097152 | tf_op jit(solution)/shard_map/all_to_all | solution.py:89
  13.9 201.9 %all-gather.2.cloned.1.call-start = ((), (), s32[]{:S(2)}) async-start(), calls=%async_computation.3 | async-start | bytes 10485760 | tf_op jit(solution)/shard_map/all_gather | solution.py:110
  14.8 35.5 %collective-permute-start = (bf16[4,64,256]{2,1,0:T(8,128)(2,1)S(1)}, bf16[4,64,256]{2,1,0:T(8,128)(2,1)}, u32[]{:S(2)}, u32[]{:S(2)}) collective-permute-start(bf16[4,64,256]{2,1,0:T(8,128)(2,1)S(1)} %get-tuple-element.226), channel_id=1, source_target_pairs={{0,4},{4,0},{8,12},{12,8},{16,20},{20,16},{24,28},{28,24},{1,5},{5... | collective-permute-start | bytes 393224 | tf_op jit(solution)/shard_map/ppermute | solution.py:27
  16.8 38.9 %collective-permute-start.1 = (bf16[4,64,256]{2,1,0:T(8,128)(2,1)S(1)}, bf16[4,64,256]{2,1,0:T(8,128)(2,1)S(1)}, u32[]{:S(2)}, u32[]{:S(2)}) collective-permute-start(bf16[4,64,256]{2,1,0:T(8,128)(2,1)S(1)} %get-tuple-element.225), channel_id=1, source_target_pairs={{0,8},{4,12},{8,0},{12,4},{16,24},{20,28},{24,16},{28,20},{1,9},{5... | collective-permute-start | bytes 393224 | tf_op jit(solution)/shard_map/ppermute | solution.py:27
  18.2 39.6 %collective-permute-start.2 = (bf16[4,64,256]{2,1,0:T(8,128)(2,1)S(1)}, bf16[4,64,256]{2,1,0:T(8,128)(2,1)S(1)}, u32[]{:S(2)}, u32[]{:S(2)}) collective-permute-start(bf16[4,64,256]{2,1,0:T(8,128)(2,1)S(1)} %get-tuple-element.224), channel_id=1, source_target_pairs={{0,12},{4,8},{8,4},{12,0},{16,28},{20,24},{24,20},{28,16},{1,13},{... | collective-permute-start | bytes 393224 | tf_op jit(solution)/shard_map/ppermute | solution.py:27
  18.3 40.1 %collective-permute-start.3 = (bf16[4,64,256]{2,1,0:T(8,128)(2,1)S(1)}, bf16[4,64,256]{2,1,0:T(8,128)(2,1)S(1)}, u32[]{:S(2)}, u32[]{:S(2)}) collective-permute-start(bf16[4,64,256]{2,1,0:T(8,128)(2,1)S(1)} %get-tuple-element.223), channel_id=1, source_target_pairs={{0,16},{4,20},{8,24},{12,28},{16,0},{20,4},{24,8},{28,12},{1,17},{... | collective-permute-start | bytes 393224 | tf_op jit(solution)/shard_map/ppermute | solution.py:27
  21.2 38.6 %collective-permute-start.4 = (bf16[4,64,256]{2,1,0:T(8,128)(2,1)S(1)}, bf16[4,64,256]{2,1,0:T(8,128)(2,1)S(1)}, u32[]{:S(2)}, u32[]{:S(2)}) collective-permute-start(bf16[4,64,256]{2,1,0:T(8,128)(2,1)S(1)} %get-tuple-element.222), channel_id=1, source_target_pairs={{0,20},{4,16},{8,28},{12,24},{16,4},{20,0},{24,12},{28,8},{1,21},{... | collective-permute-start | bytes 393224 | tf_op jit(solution)/shard_map/ppermute | solution.py:27
  46.7 33.8 %all-to-all-start.1 = ((bf16[32,64,256]{2,1,0:T(8,128)(2,1)}), bf16[32,64,256]{2,1,0:T(8,128)(2,1)S(1)}, u32[]{:S(2)}, u32[]{:S(2)}) async-start(bf16[32,64,256]{2,1,0:T(8,128)(2,1)} %bitcast.4), calls=%async_computation.1 | async-start | bytes 2097152 | tf_op jit(solution)/shard_map/all_to_all | solution.py:86
  50.3 19.8 %collective-permute-start.5 = (bf16[4,64,256]{2,1,0:T(8,128)(2,1)S(1)}, bf16[4,64,256]{2,1,0:T(8,128)(2,1)S(1)}, u32[]{:S(2)}, u32[]{:S(2)}) collective-permute-start(bf16[4,64,256]{2,1,0:T(8,128)(2,1)S(1)} %get-tuple-element.221), channel_id=1, source_target_pairs={{0,24},{4,28},{8,16},{12,20},{16,8},{20,12},{24,0},{28,4},{1,25},{... | collective-permute-start | bytes 393224 | tf_op jit(solution)/shard_map/ppermute | solution.py:27
  55.7 16.9 %collective-permute-start.6 = (bf16[4,64,256]{2,1,0:T(8,128)(2,1)S(1)}, bf16[4,64,256]{2,1,0:T(8,128)(2,1)S(1)}, u32[]{:S(2)}, u32[]{:S(2)}) collective-permute-start(bf16[4,64,256]{2,1,0:T(8,128)(2,1)S(1)} %get-tuple-element.220), channel_id=1, source_target_pairs={{0,28},{4,24},{8,20},{12,16},{16,12},{20,8},{24,4},{28,0},{1,29},{... | collective-permute-start | bytes 393224 | tf_op jit(solution)/shard_map/ppermute | solution.py:27
  102.6 1.2 copy-start
  126.0 1.2 copy-start
  149.4 1.2 copy-start
  172.7 1.2 copy-start
Sparse Core Ops, SparseCore 0:
  22.8 58.2 all-gather.1
